TPU v7x, 32 devices: a whole 2x2x4 slice. The times are simulated.
32 devices in a mesh: grp: 2 (over x), kv: 4 (over y, core), tp: 4 (over z).
Axes of the slice: x: 2, y: 2, z: 4, core: 2. Of those that a mesh axis runs over, the one named last changes fastest.
Arguments:
- tokens: bfloat16 [128, 4096], P('grp', ('kv', 'tp')), parts along dimension 0, may hold values from -20 to 20, as said below
- norm_gain: bfloat16 [4096], P('kv'), may hold values from 0.099609375 to 1.8984375
- w_query: bfloat16 [4096, 2048], P('kv', 'tp'), may hold values from -0.09375 to 0.09375
- w_key: bfloat16 [4096, 2048], P('kv', 'tp'), may hold values from -0.09375 to 0.09375
- w_value: bfloat16 [4096, 4096], P('kv', 'tp'), may hold values from -0.09375 to 0.09375
- w_outgate: bfloat16 [4096, 4096], P('kv', 'tp'), may hold values from -0.09375 to 0.09375
- w_input_gate: bfloat16 [4096, 32], P('kv'), may hold values from -0.09375 to 0.09375
- w_forget_gate: bfloat16 [4096, 32], P('kv'), may hold values from -0.09375 to 0.09375
- memory: float32 [128, 32, 64, 128], P(('grp', 'kv'), 'tp'), parts along dimension 0, may hold values from -4 to 4
- normalizer: float32 [128, 32, 64], P(('grp', 'kv'), 'tp'), parts along dimension 0, may hold values from -4 to 4
- stabilizer: float32 [128, 32], P(('grp', 'kv'), 'tp'), parts along dimension 0, may hold values from -4 to 4
- w_mix_out: bfloat16 [4096, 4096], P('tp', 'kv'), may hold values from -0.09375 to 0.09375
- ffn_gain: bfloat16 [4096], P('kv'), may hold values from 0.099609375 to 1.8984375
- w_gate: bfloat16 [4096, 11264], P('kv', 'tp'), may hold values from -0.09375 to 0.09375
- w_up: bfloat16 [4096, 11264], P('kv', 'tp'), may hold values from -0.09375 to 0.09375
- w_down: bfloat16 [11264, 4096], P('tp', 'kv'), may hold values from -0.3125 to 0.3125
Outputs:
- layer_out: bfloat16 [128, 4096], P('grp', ('kv', 'tp')), parts along dimension 0
- new_memory: float32 [128, 32, 64, 128], P(('grp', 'kv'), 'tp'), parts along dimension 0
- new_normalizer: float32 [128, 32, 64], P(('grp', 'kv'), 'tp'), parts along dimension 0
- new_stabilizer: float32 [128, 32], P(('grp', 'kv'), 'tp'), parts along dimension 0
There are 2 independent parts, one for each index of `grp`. A program takes and returns all parts, laid end to end along the dimension named above; an argument that names none is the same for every part. Nothing has to cross between parts.
Inputs may be any that keep to these rules, and one draw needn't show every extreme that they name: tokens' feature scales differ by column and by sequence.
All inputs are finite; a program needn't handle non-finite values.
Results may differ from a plain program's by a relative error of at most 0.029.
Values may be sent and summed in bfloat16 or wider, within the bound.
A program may use at most 64 MiB of HBM per device.

v0:
```python
import jax
import jax.numpy as jnp
from jax import lax
from jax.sharding import PartitionSpec as P

D = 4096
DQK = 64
DV = 128


def shards(
    tokens,
    norm_gain,
    w_query,
    w_key,
    w_value,
    w_outgate,
    w_input_gate,
    w_forget_gate,
    memory,
    normalizer,
    stabilizer,
    w_mix_out,
    ffn_gain,
    w_gate,
    w_up,
    w_down,
):
    seqs = tokens.shape[0]
    weights = (w_query, w_key, w_value, w_outgate, w_input_gate, w_forget_gate)
    start_proj = tuple((jnp.zeros((seqs, weight.shape[1]), jnp.float32) for weight in weights))
    start_proj = start_proj + (jnp.zeros((seqs,), jnp.float32),)
    wide = lax.all_gather(tokens, "tp", axis=1, tiled=True).astype(jnp.float32)
    gain = norm_gain.astype(jnp.float32)
    normed = (wide * gain[None, :]).astype(jnp.bfloat16)
    sums = tuple(
        (jnp.dot(normed, weight, preferred_element_type=jnp.float32) for weight in weights)
    )
    totals = sums + (jnp.sum(wide * wide, axis=1),)
    z_query, z_key, z_value, z_outgate, z_input, z_forget, squares = lax.psum_scatter(
        totals, "kv", scatter_dimension=0, tiled=True
    )
    own = z_query.shape[0]
    local_heads = memory.shape[1]
    scale1 = lax.rsqrt(squares / D + 1e-06)
    head_start = lax.axis_index("tp") * local_heads
    query = (scale1[:, None] * z_query).reshape(own, local_heads, DQK) * DQK ** (-0.5)
    key = (scale1[:, None] * z_key).reshape(own, local_heads, DQK)
    value = (scale1[:, None] * z_value).reshape(own, local_heads, DV)
    outgate = scale1[:, None] * z_outgate
    igate = scale1[:, None] * lax.dynamic_slice_in_dim(z_input, head_start, local_heads, 1)
    lforget = jax.nn.log_sigmoid(
        scale1[:, None] * lax.dynamic_slice_in_dim(z_forget, head_start, local_heads, 1)
    )
    new_stabilizer = jnp.maximum(lforget + stabilizer, igate)
    decay = jnp.exp(lforget + stabilizer - new_stabilizer)
    inflow = jnp.exp(igate - new_stabilizer)
    new_memory = (
        decay[:, :, None, None] * memory
        + inflow[:, :, None, None] * key[:, :, :, None] * value[:, :, None, :]
    )
    new_normalizer = decay[:, :, None] * normalizer + inflow[:, :, None] * key
    numer = jnp.einsum("bhd,bhde->bhe", query, new_memory)
    denom = jnp.sum(query * new_normalizer, axis=-1)
    readout = numer / jnp.maximum(jnp.abs(denom), jnp.exp(-new_stabilizer))[:, :, None]
    gated = (jax.nn.sigmoid(outgate) * readout.reshape(own, local_heads * DV)).astype(jnp.bfloat16)
    mix_partial = jnp.dot(
        lax.all_gather(gated, "kv", axis=0, tiled=True),
        w_mix_out,
        preferred_element_type=jnp.float32,
    )
    mix_total = lax.psum_scatter(
        mix_partial.astype(jnp.bfloat16), "tp", scatter_dimension=1, tiled=True
    ).astype(jnp.float32)
    mixed_in = (tokens.astype(jnp.float32) + mix_total).astype(jnp.bfloat16)
    wide = lax.all_gather(mixed_in, "tp", axis=1, tiled=True).astype(jnp.float32)
    gain = ffn_gain.astype(jnp.float32)
    normed = (wide * gain[None, :]).astype(jnp.bfloat16)
    gate_sum = jnp.dot(normed, w_gate, preferred_element_type=jnp.float32)
    up_sum = jnp.dot(normed, w_up, preferred_element_type=jnp.float32)
    gate_part = gate_sum
    up_part = up_sum
    square_part = jnp.sum(wide * wide, axis=1)
    gate_sum, up_sum, square_sum = lax.psum((gate_part, up_part, square_part), "kv")
    scale2 = lax.rsqrt(square_sum / D + 1e-06)[:, None]
    hidden = (jax.nn.silu(scale2 * gate_sum) * (scale2 * up_sum)).astype(jnp.bfloat16)
    down_partial = jnp.dot(hidden, w_down, preferred_element_type=jnp.float32)
    down_total = lax.psum_scatter(
        down_partial.astype(jnp.bfloat16), "tp", scatter_dimension=1, tiled=True
    ).astype(jnp.float32)
    layer_out = (mixed_in.astype(jnp.float32) + down_total).astype(jnp.bfloat16)
    return (layer_out, new_memory, new_normalizer, new_stabilizer)


def solution(mesh):
    in_specs = (
        P("grp", ("kv", "tp")),
        P("kv"),
        P("kv", "tp"),
        P("kv", "tp"),
        P("kv", "tp"),
        P("kv", "tp"),
        P("kv", None),
        P("kv", None),
        P(("grp", "kv"), "tp", None, None),
        P(("grp", "kv"), "tp", None),
        P(("grp", "kv"), "tp"),
        P("tp", "kv"),
        P("kv"),
        P("kv", "tp"),
        P("kv", "tp"),
        P("tp", "kv"),
    )
    out_specs = (
        P("grp", ("kv", "tp")),
        P(("grp", "kv"), "tp", None, None),
        P(("grp", "kv"), "tp", None),
        P(("grp", "kv"), "tp"),
    )
    return jax.shard_map(shards, mesh=mesh, in_specs=in_specs, out_specs=out_specs, check_vma=False)
```

profile of v0, /device:TPU:0, one launch (start us, length us, event | category | flops | bytes accessed | tf_op | source)
XLA Modules:
  0.0 282.0 jit_solution(5169537857408966989)
XLA Ops:
  7.2 0.0 reduce-scatter.13.cloned.1.call-start
  7.2 0.8 convert_element_type.50
  8.1 15.3 %all_gather.9 = bf16[64,1024]{1,0:T(8,128)(2,1)S(1)} all-gather(bf16[64,256]{1,0:T(8,128)(2,1)} %param.16), channel_id=1, replica_groups=mesh['grp'=2,'kv'=4,'tp'=4] {'tp'}, dimensions={1}, use_global_device_ids=true | all-gather | bytes 163840 | tf_op jit(solution)/shard_map/all_gather | solution.py:33
  23.3 1.6 fusion.17
  25.0 0.0 reduce-scatter.13.cloned.1.call-update
  25.0 0.0 reduce-scatter.15.cloned.1.call-start
  25.0 1.6 fusion.15
  26.7 0.0 reduce-scatter.15.cloned.1.call-update
  26.7 0.0 reduce-scatter.11.cloned.1.call-start
  26.8 2.2 fusion.19
  28.9 0.0 reduce-scatter.11.cloned.1.call-update
  29.0 0.0 reduce-scatter.17.cloned.1.call-start
  29.0 2.2 fusion.13
  31.2 0.0 reduce-scatter.17.cloned.1.call-update
  31.2 0.0 reduce-scatter.19.cloned.1.call-start
  31.3 1.2 fusion.11
  32.5 0.0 reduce-scatter.19.cloned.1.call-update
  32.5 0.0 reduce-scatter.9.cloned.1.call-start
  32.5 2.8 fusion.21
  35.3 0.0 reduce-scatter.9.cloned.1.call-update
  35.3 0.0 reduce-scatter.21.cloned.1.call-start
  35.4 0.1 fusion.2
  35.5 0.1 copy.22
  35.6 5.6 %all-reduce = f32[64]{0:T(128)S(1)} all-reduce(f32[64]{0:T(128)S(1)} %fusion.2), channel_id=2, replica_groups=mesh['grp'=2,'kv'=4,'tp'=4] {'kv'}, use_global_device_ids=true, to_apply=%region_1.0.clone | all-reduce | flops 64 | bytes 512
  41.2 0.6 dynamic-slice
  42.5 0.1 fusion.27
  42.5 3.5 %reduce-scatter.13.cloned.1.call-done = f32[16,32]{1,0:T(8,128)} async-done(((f32[64,32]{1,0:T(8,128)}), f32[16,32]{1,0:T(8,128)}) %reduce-scatter.13.cloned.1.call-update) | async-done | bytes 2064 | tf_op jit(solution)/shard_map/reduce_scatter | solution.py:40
  46.1 22.6 %reduce-scatter.15.cloned.1.call-done = f32[16,32]{1,0:T(8,128)} async-done(((f32[64,32]{1,0:T(8,128)}), f32[16,32]{1,0:T(8,128)}) %reduce-scatter.15.cloned.1.call-update) | async-done | bytes 2064 | tf_op jit(solution)/shard_map/reduce_scatter | solution.py:40
  68.6 0.8 subtract_exponential_fusion.1
  69.4 0.8 subtract_exponential_fusion
  70.2 20.5 %reduce-scatter.11.cloned.1.call-done = f32[16,512]{1,0:T(8,128)} async-done(((f32[64,512]{1,0:T(8,128)}), f32[16,512]{1,0:T(8,128)}) %reduce-scatter.11.cloned.1.call-update) | async-done | bytes 32784 | tf_op jit(solution)/shard_map/reduce_scatter | solution.py:40
  90.7 22.0 %reduce-scatter.17.cloned.1.call-done = f32[16,512]{1,0:T(8,128)} async-done(((f32[64,512]{1,0:T(8,128)}), f32[16,512]{1,0:T(8,128)}) %reduce-scatter.17.cloned.1.call-update) | async-done | bytes 32784 | tf_op jit(solution)/shard_map/reduce_scatter | solution.py:40
  112.7 0.8 broadcast_multiply_fusion.1
  113.6 0.1 reshape.35
  113.6 0.1 mul.160
  113.7 0.1 broadcast_in_dim_reshape.4
  113.8 0.7 multiply_reduce_fusion
  114.5 21.1 %reduce-scatter.19.cloned.1.call-done = f32[16,1024]{1,0:T(8,128)} async-done(((f32[64,1024]{1,0:T(8,128)}), f32[16,1024]{1,0:T(8,128)}) %reduce-scatter.19.cloned.1.call-update) | async-done | bytes 65552 | tf_op jit(solution)/shard_map/reduce_scatter | solution.py:40
  135.7 0.9 multiply_bitcast_fusion
  136.6 3.7 %multiply_add_fusion = f32[16,8,64,128]{3,2,1,0:T(8,128)S(1)} fusion(f32[16,8,64,128]{3,2,1,0:T(8,128)} %param.24, f32[16,8,128]{2,1,0:T(8,128)S(1)} %bitcast.26, f32[16,8,64]{2,1,0:T(8,128)S(1)} %get-tuple-element.16, f32[16,8]{1,0:T(8,128)S(1)} %get-tuple-element.17), kind=kLoop, calls=%fused_computation | loop fusion | flops 3145728 | bytes 8487424 | tf_op jit(solution)/shard_map/add | solution.py:59
  140.4 2.0 copy-done.1
  142.4 0.7 fusion.30
  143.0 0.1 broadcast_divide_fusion
  143.1 14.9 %reduce-scatter.9.cloned.1.call-done = f32[16,1024]{1,0:T(8,128)} async-done(((f32[64,1024]{1,0:T(8,128)}), f32[16,1024]{1,0:T(8,128)}) %reduce-scatter.9.cloned.1.call-update) | async-done | bytes 65552 | tf_op jit(solution)/shard_map/reduce_scatter | solution.py:40
  158.1 0.9 fusion.10
  159.0 5.4 %all_gather.10 = bf16[64,1024]{1,0:T(8,128)(2,1)S(1)} all-gather(bf16[16,1024]{1,0:T(8,128)(2,1)S(1)} %fusion.10), channel_id=1, replica_groups=mesh['grp'=2,'kv'=4,'tp'=4] {'kv'}, dimensions={0}, use_global_device_ids=true | all-gather | bytes 163840 | tf_op jit(solution)/shard_map/all_gather | solution.py:68
  164.4 2.7 convolution_convert_fusion
  167.1 0.0 reduce-scatter.21.cloned.1.call-update
  167.2 0.0 all-reduce.4.cloned.1.call-start
  167.2 19.5 %reduce-scatter.21.cloned.1.call-done = bf16[64,256]{1,0:T(8,128)(2,1)} async-done(((bf16[64,1024]{1,0:T(8,128)(2,1)}), bf16[64,256]{1,0:T(8,128)(2,1)}) %reduce-scatter.21.cloned.1.call-update) | async-done | bytes 32784 | tf_op jit(solution)/shard_map/reduce_scatter | solution.py:72
  186.8 0.8 add_convert_fusion.1
  187.5 13.3 %all_gather.11 = bf16[64,1024]{1,0:T(8,128)(2,1)S(1)} all-gather(bf16[64,256]{1,0:T(8,128)(2,1)S(1)} %add_convert_fusion.1), channel_id=1, replica_groups=mesh['grp'=2,'kv'=4,'tp'=4] {'tp'}, dimensions={1}, use_global_device_ids=true | all-gather | bytes 163840 | tf_op jit(solution)/shard_map/all_gather | solution.py:76
  200.9 4.6 %fusion.6 = f32[64,2816]{1,0:T(8,128)} fusion(bf16[1024,2816]{1,0:T(8,128)(2,1)} %param.30, bf16[64,1024]{1,0:T(8,128)(2,1)S(1)} %all_gather.11, f32[1024]{0:T(1024)S(1)} %convert_element_type.58), kind=kOutput, calls=%fused_computation.14 | convolution fusion | flops 369295360 | bytes 6623232 | tf_op jit(solution)/shard_map/dot_general | solution.py:80
  205.5 4.6 %fusion.8 = f32[64,2816]{1,0:T(8,128)} fusion(bf16[1024,2816]{1,0:T(8,128)(2,1)} %param.29, bf16[64,1024]{1,0:T(8,128)(2,1)S(1)} %all_gather.11, f32[1024]{0:T(1024)S(1)} %convert_element_type.58), kind=kOutput, calls=%fused_computation.15 | convolution fusion | flops 369295360 | bytes 6623232 | tf_op jit(solution)/shard_map/dot_general | solution.py:79
  210.1 0.0 all-reduce.4.cloned.1.call-update
  210.2 0.0 reduce-scatter.23.cloned.1.call-start
  210.2 0.1 fusion.4
  210.3 5.7 %psum.21 = f32[64]{0:T(128)S(1)} all-reduce(f32[64]{0:T(128)S(1)} %fusion.4), channel_id=1, replica_groups=mesh['grp'=2,'kv'=4,'tp'=4] {'kv'}, use_global_device_ids=true, to_apply=%region_11.12 | all-reduce | flops 64 | bytes 512 | tf_op jit(solution)/shard_map/psum | solution.py:84
  216.0 33.5 %all-reduce.4.cloned.1.call-done = (f32[64,2816]{1,0:T(8,128)}, f32[64,2816]{1,0:T(8,128)}) async-done(((f32[64,2816]{1,0:T(8,128)}, f32[64,2816]{1,0:T(8,128)}), (f32[64,2816]{1,0:T(8,128)}, f32[64,2816]{1,0:T(8,128)})) %all-reduce.4.cloned.1.call-update) | async-done | bytes 1441808 | tf_op jit(solution)/shard_map/psum | solution.py:84
  249.5 4.9 %convolution_convert_fusion.1 = bf16[64,1024]{1,0:T(8,128)(2,1)} fusion(bf16[2816,1024]{1,0:T(8,128)(2,1)} %param.31, f32[64,2816]{1,0:T(8,128)} %get-tuple-element.12, f32[64,2816]{1,0:T(8,128)} %get-tuple-element.13, f32[64]{0:T(128)S(1)} %add_rsqrt_fusion), kind=kOutput, calls=%fused_computation.2 | convolution fusion | flops 370606080 | bytes 7340288 | tf_op jit(solution)/shard_map/dot_general | solution.py:87
  254.4 0.0 reduce-scatter.23.cloned.1.call-update
  254.4 0.7 copy.23
  255.1 19.0 %reduce-scatter.23.cloned.1.call-done = bf16[64,256]{1,0:T(8,128)(2,1)} async-done(((bf16[64,1024]{1,0:T(8,128)(2,1)}), bf16[64,256]{1,0:T(8,128)(2,1)}) %reduce-scatter.23.cloned.1.call-update) | async-done | bytes 32784 | tf_op jit(solution)/shard_map/reduce_scatter | solution.py:88
  274.1 1.4 add_convert_fusion
  (17 shorter events, 0.1 us)
Async XLA Ops:
  7.2 24.1 %copy-start = (bf16[1024,1024]{1,0:T(8,128)(2,1)S(1)}, bf16[1024,1024]{1,0:T(8,128)(2,1)}, u32[]{:S(2)}) copy-start(bf16[1024,1024]{1,0:T(8,128)(2,1)} %param.20) | copy-start | bytes 6291460
  7.2 38.9 %reduce-scatter.13.cloned.1.call-start = ((), (), s32[]{:S(2)}) async-start(), calls=%async_computation.10 | async-start | bytes 40960 | tf_op jit(solution)/shard_map/reduce_scatter | solution.py:40
  25.0 43.6 %reduce-scatter.15.cloned.1.call-start = ((), (), s32[]{:S(2)}) async-start(), calls=%async_computation.11 | async-start | bytes 40960 | tf_op jit(solution)/shard_map/reduce_scatter | solution.py:40
  26.7 8.8 %copy-start.4 = (f32[16,8]{0,1:T(8,128)S(1)}, f32[16,8]{0,1:T(8,128)}, u32[]{:S(2)}) copy-start(f32[16,8]{0,1:T(8,128)} %param.26) | copy-start | bytes 1540
  26.7 14.5 %copy-start.6 = (u32[32]{0:T(128)S(1)}, u32[32]{0:T(128)}, u32[]{:S(2)}) copy-start(u32[32]{0:T(128)} %constant.31) | copy-start | bytes 388
  26.7 64.0 %reduce-scatter.11.cloned.1.call-start = ((), (), s32[]{:S(2)}) async-start(), calls=%async_computation.9 | async-start | bytes 163840 | tf_op jit(solution)/shard_map/reduce_scatter | solution.py:40
  28.9 84.9 %copy-start.3 = (f32[16,8,64]{2,1,0:T(8,128)S(1)}, f32[16,8,64]{2,1,0:T(8,128)}, u32[]{:S(2)}) copy-start(f32[16,8,64]{2,1,0:T(8,128)} %param.25) | copy-start | bytes 98308
  29.0 83.8 %reduce-scatter.17.cloned.1.call-start = ((), (), s32[]{:S(2)}) async-start(), calls=%async_computation.12 | async-start | bytes 163840 | tf_op jit(solution)/shard_map/reduce_scatter | solution.py:40
  31.2 104.5 %reduce-scatter.19.cloned.1.call-start = ((), (), s32[]{:S(2)}) async-start(), calls=%async_computation.13 | async-start | bytes 327680 | tf_op jit(solution)/shard_map/reduce_scatter | solution.py:40
  32.5 125.6 %reduce-scatter.9.cloned.1.call-start = ((), (), s32[]{:S(2)}) async-start(), calls=%async_computation.8 | async-start | bytes 327680 | tf_op jit(solution)/shard_map/reduce_scatter | solution.py:40
  35.3 151.4 %reduce-scatter.21.cloned.1.call-start = ((), (), s32[]{:S(2)}) async-start(), calls=%async_computation.14 | async-start | bytes 163840 | tf_op jit(solution)/shard_map/reduce_scatter | solution.py:72
  140.4 2.0 copy-start.1
  140.4 26.9 %copy-start.5 = (bf16[1024]{0:T(1024)(128)(2,1)S(1)}, bf16[1024]{0:T(1024)(128)(2,1)}, u32[]{:S(2)}) copy-start(bf16[1024]{0:T(1024)(128)(2,1)} %param.28) | copy-start | bytes 6148
  140.4 46.4 %copy-start.2 = (bf16[64,256]{1,0:T(8,128)(2,1)S(1)}, bf16[64,256]{1,0:T(8,128)(2,1)}, u32[]{:S(2)}) copy-start(bf16[64,256]{1,0:T(8,128)(2,1)} %param.16) | copy-start | bytes 98308
  167.2 82.3 %all-reduce.4.cloned.1.call-start = ((), (), s32[]{:S(2)}) async-start(), calls=%async_computation.16 | async-start | bytes 2883584 | tf_op jit(solution)/shard_map/psum | solution.py:84
  210.2 63.9 %reduce-scatter.23.cloned.1.call-start = ((), (), s32[]{:S(2)}) async-start(), calls=%async_computation.15 | async-start | bytes 163840 | tf_op jit(solution)/shard_map/reduce_scatter | solution.py:88
Sparse Core Ops, SparseCore 0:
  25.1 20.9 reduce-scatter.12
  49.0 19.5 reduce-scatter.14
  71.1 19.6 reduce-scatter.10
  93.0 19.6 reduce-scatter.16
  115.6 20.0 reduce-scatter.18
  138.0 20.0 reduce-scatter.8
  167.3 19.4 reduce-scatter.20
  210.3 39.1 all-reduce.3
  254.5 19.4 reduce-scatter.22
where the time goes:
time: 283 us; the launch traced here: 282 us
  waiting for transfers between devices  177 us (63%)
  blocking collectives  45.3 us (16%)
  matrix products  29.1 us (10%)
  between operations  14.6 us (5%)
  other arithmetic  12.2 us (4%)
  local copies, waits for them, and re-layouts  3.59 us (1%)
    reduce_scatter x6, waiting for transfers between devices, shards(): lax.psum_scatter(totals, 'kv', scatter_dimension=0, tiled=True)  105 us
    psum x1, waiting for transfers between devices, shards(): lax.psum((gate_part, up_part, square_part), 'kv')  33.5 us
    reduce_scatter x1, waiting for transfers between devices, shards(): lax.psum_scatter(mix_partial.astype(jnp.bfloat16), 'tp', scatter_dimensio...  19.5 us
    reduce_scatter x1, waiting for transfers between devices, shards(): lax.psum_scatter(down_partial.astype(jnp.bfloat16), 'tp', scatter_dimensi...  19 us
    all_gather x1, blocking collectives, shards(): wide = lax.all_gather(tokens, 'tp', axis=1, tiled=True).astype(jnp.float32)  15.3 us
    all_gather x1, blocking collectives, shards(): lax.all_gather(mixed_in, 'tp', axis=1, tiled=True).astype(jnp.float32)  13.3 us
    dot_general x6, matrix products, shards(): jnp.dot(normed, weight, preferred_element_type=jnp.float32)  11.6 us
    psum x1, blocking collectives, shards(): lax.psum((gate_part, up_part, square_part), 'kv')  5.66 us
  transfers between devices with their start and end apart: 9, of which 9 were waited for; matrix products, arithmetic and copies ran while one was open for 7% of the time, Pallas kernels for 0%

commit v1 on v0

v1 whole, which is shorter than its diff:
```python
import functools

import jax
import jax.numpy as jnp
from jax import lax
from jax.experimental import pallas as pl
from jax.experimental.pallas import tpu as pltpu
from jax.sharding import PartitionSpec as P

D = 4096
DQK = 64
DV = 128
F32 = jnp.float32
BF16 = jnp.bfloat16
MESH = pl.DeviceIdType.MESH
VMEM_LIMIT = 60 * 1024 * 1024


def remote(src, dst, send_sem, recv_sem, **device):
    return pltpu.make_async_remote_copy(
        src_ref=src, dst_ref=dst, send_sem=send_sem, recv_sem=recv_sem,
        device_id=device, device_id_type=MESH,
    )


class Place:
    def __init__(self, nkv, ntp):
        self.nkv, self.ntp, self.ny = nkv, ntp, nkv // 2
        self.kv = lax.axis_index("kv")
        self.tp = lax.axis_index("tp")
        self.y = self.kv // 2
        self.core = self.kv % 2
        self.pending = []

    def mate(self):
        return 2 * self.y + (1 - self.core)

    def barrier(self):
        sem = pltpu.get_barrier_semaphore()
        count = 0
        for d in range(1, self.ntp):
            pl.semaphore_signal(sem, inc=1, device_id={"tp": (self.tp + d) % self.ntp}, device_id_type=MESH)
            count += 1
        pl.semaphore_signal(sem, inc=1, device_id={"kv": self.mate()}, device_id_type=MESH)
        count += 1
        for d in range(1, self.ny):
            other = 2 * ((self.y + d) % self.ny) + self.core
            pl.semaphore_signal(sem, inc=1, device_id={"kv": other}, device_id_type=MESH)
            count += 1
        pl.semaphore_wait(sem, count)

    def send(self, copy):
        copy.start()
        self.pending.append(copy)

    def finish(self):
        for copy in self.pending:
            copy.wait_send()

    def tp_send_all(self, src_of, slots, ssem, rsem):
        for d in range(1, self.ntp):
            to = (self.tp + d) % self.ntp
            self.send(remote(src_of(to), slots.at[self.tp], ssem.at[to], rsem.at[self.tp], tp=to))

    def tp_wait_all(self, slots, ssem, rsem):
        for d in range(1, self.ntp):
            to = (self.tp + self.ntp - d) % self.ntp
            remote(slots.at[to], slots.at[to], ssem.at[to], rsem.at[to], tp=to).wait_recv()


class Scatter:
    def __init__(self, place, acc, r1, s2, r2, sems, g):
        self.p, self.acc, self.r1, self.s2, self.r2 = place, acc, r1, s2, r2
        self.d_s, self.d_r, self.y_s, self.y_r = (s.at[g] for s in sems)

    def start(self):
        p = self.p
        for d in range(1, p.ny + 1):
            y = (p.y + d) % p.ny
            p.send(remote(self.acc.at[2 * y + (1 - p.core)], self.r1.at[y], self.d_s.at[y], self.d_r.at[y], kv=p.mate()))

    def chip_sum(self, y):
        p = self.p
        remote(self.r1.at[y], self.r1.at[y], self.d_s.at[y], self.d_r.at[y], kv=p.mate()).wait_recv()
        return self.acc[2 * y + p.core] + self.r1[y]

    def middle(self):
        p = self.p
        for d in range(1, p.ny):
            y = (p.y + d) % p.ny
            self.s2[y] = self.chip_sum(y).astype(self.s2.dtype)
            p.send(remote(self.s2.at[y], self.r2.at[p.y], self.y_s.at[y], self.y_r.at[p.y], kv=2 * y + p.core))

    def end(self):
        p = self.p
        total = self.chip_sum(p.y)
        for d in range(1, p.ny):
            y = (p.y + p.ny - d) % p.ny
            remote(self.r2.at[y], self.r2.at[y], self.y_s.at[y], self.y_r.at[y], kv=2 * y + p.core).wait_recv()
            total = total + self.r2[y].astype(F32)
        return total


def scatter_scratch(nkv, own, n, dtype):
    ny = nkv // 2
    return [
        pltpu.VMEM((nkv, own, n), F32),
        pltpu.VMEM((ny, own, n), F32),
        pltpu.VMEM((ny, own, n), dtype),
        pltpu.VMEM((ny, own, n), dtype),
    ]


def scatter_sems(groups, ny):
    return [pltpu.SemaphoreType.DMA((groups, ny))] * 4


class Gather:
    def __init__(self, place, slots, sems, g):
        self.p, self.slots = place, slots
        self.y_s, self.y_r, self.d_s, self.d_r = (s.at[g] for s in sems)

    def start(self):
        p, mine = self.p, self.slots.at[self.p.kv]
        for d in range(1, p.ny):
            y = (p.y + d) % p.ny
            p.send(remote(mine, mine, self.y_s.at[y], self.y_r.at[p.y], kv=2 * y + p.core))
        p.send(remote(mine, mine, self.d_s.at[p.y], self.d_r.at[p.y], kv=p.mate()))

    def relay(self):
        p = self.p
        for d in range(1, p.ny):
            y = (p.y + p.ny - d) % p.ny
            slot = self.slots.at[2 * y + p.core]
            remote(slot, slot, self.y_s.at[y], self.y_r.at[y], kv=2 * y + p.core).wait_recv()
            p.send(remote(slot, slot, self.d_s.at[y], self.d_r.at[y], kv=p.mate()))

    def end(self):
        p = self.p
        for d in range(p.ny):
            y = (p.y + p.ny - d) % p.ny
            slot = self.slots.at[2 * y + 1 - p.core]
            remote(slot, slot, self.d_s.at[y], self.d_r.at[y], kv=p.mate()).wait_recv()


def normalize(place, pieces, gain, normed):
    cw = pieces.shape[2]
    squares = None
    for t in range(place.ntp):
        wide = pieces[t].astype(F32)
        normed[:, t * cw:(t + 1) * cw] = (wide * gain[:, t * cw:(t + 1) * cw].astype(F32)).astype(BF16)
        part = jnp.sum(wide * wide, axis=1, keepdims=True)
        squares = part if squares is None else squares + part
    return squares


def load(pairs, sems):
    copies = [pltpu.make_async_copy(src, dst, sems.at[i]) for i, (src, dst) in enumerate(pairs)]
    for copy in copies:
        copy.start()
    return copies


def project_kernel(nkv, ntp, tokens, gain, *refs):
    hbm, outs, refs = refs[:6], refs[6:11], refs[11:]
    vmem, (pieces, normed, load_sem, tp_s, tp_r), refs = refs[:6], refs[6:11], refs[11:]
    groups, sems = refs[:20], refs[20:24]
    own = tokens.shape[0] // nkv
    loads = load(list(zip(hbm, vmem)), load_sem)
    place = Place(nkv, ntp)
    place.barrier()
    place.tp_send_all(lambda to: tokens, pieces, tp_s, tp_r)
    pieces[place.tp] = tokens[...]
    place.tp_wait_all(pieces, tp_s, tp_r)
    squares = normalize(place, pieces, gain, normed)
    scatters = [Scatter(place, *groups[4 * g:4 * g + 4], sems, g) for g in range(5)]

    def split(value):
        return value.reshape(nkv, own, value.shape[1])

    small = groups[16]
    nh = vmem[4].shape[1]
    small[:, :, 2 * nh:] = split(jnp.broadcast_to(squares, (nkv * own, small.shape[2] - 2 * nh)))
    for g, at in ((4, 0), (5, nh)):
        loads[g].wait()
        small[:, :, at:at + nh] = split(jnp.dot(normed[...], vmem[g][...], preferred_element_type=F32))
    scatters[4].start()
    for g in range(4):
        loads[g].wait()
        groups[4 * g][...] = split(jnp.dot(normed[...], vmem[g][...], preferred_element_type=F32))
        scatters[g].start()
        scatters[g - 1 if g else 4].middle()
    scatters[3].middle()
    for g in (4, 0, 1, 2, 3):
        outs[g][...] = scatters[g].end()
    place.finish()


def mixer_kernel(nkv, ntp, chunks, gated, tokens, gain, *refs):
    hbm, out, refs = refs[:4], refs[4], refs[5:]
    (w_mix, w_gate, w_up, w_down), refs = refs[:4], refs[4:]
    (g_all, m_out, m_in, mine, pieces, normed, d_out, d_in, total, load_sem), refs = refs[:10], refs[10:]
    m_s, m_r, x_s, x_r, l_s, l_r = refs[:6]
    refs = refs[6:]
    n = len(chunks)
    small, refs = refs[:4], refs[4:]
    groups, refs = refs[:4 * n], refs[4 * n:]
    halls, refs = refs[:n], refs[n:]
    scatter_s, gather_s = refs[:4], refs[4:8]
    rows, cw = tokens.shape
    own = rows // nkv
    wide_n = nkv * own

    loads = load(list(zip(hbm, (w_mix, w_gate, w_up, w_down))), load_sem)
    place = Place(nkv, ntp)
    g_all[place.kv] = gated[...]
    place.barrier()
    first = Gather(place, g_all, gather_s, n)
    first.start()
    first.relay()
    first.end()
    loads[0].wait()

    def scatter_tp(value, outgoing, incoming, ssem, rsem):
        for t in range(ntp):
            outgoing[t] = value[:, t * cw:(t + 1) * cw].astype(BF16)
        place.tp_send_all(lambda to: outgoing.at[to], incoming, ssem, rsem)
        place.tp_wait_all(incoming, ssem, rsem)
        result = outgoing[place.tp].astype(F32)
        for d in range(1, ntp):
            result = result + incoming[(place.tp + d) % ntp].astype(F32)
        return result

    mix = jnp.dot(g_all[...].reshape(wide_n, g_all.shape[2]), w_mix[...], preferred_element_type=F32)
    mixed = (tokens[...].astype(F32) + scatter_tp(mix, m_out, m_in, m_s, m_r)).astype(BF16)
    mine[...] = mixed
    pieces[place.tp] = mixed
    place.tp_send_all(lambda to: mine, pieces, x_s, x_r)
    place.tp_wait_all(pieces, x_s, x_r)
    squares = normalize(place, pieces, gain, normed)
    small[0][...] = jnp.broadcast_to(squares, (wide_n, small[0].shape[2])).reshape(nkv, own, small[0].shape[2])
    sq = Scatter(place, *small, scatter_s, n)
    sq.start()
    loads[1].wait()
    loads[2].wait()
    scatters = [Scatter(place, *groups[4 * i:4 * i + 4], scatter_s, i) for i in range(n)]
    gathers = [Gather(place, halls[i], gather_s, i) for i in range(n)]
    for i, (at, w) in enumerate(chunks):
        acc = groups[4 * i]
        acc[:, :, :w] = jnp.dot(normed[...], w_gate[:, at:at + w], preferred_element_type=F32).reshape(nkv, own, w)
        acc[:, :, w:] = jnp.dot(normed[...], w_up[:, at:at + w], preferred_element_type=F32).reshape(nkv, own, w)
        scatters[i].start()
        if i == 0:
            sq.middle()
        else:
            scatters[i - 1].middle()
    scatters[n - 1].middle()
    scale2 = lax.rsqrt(sq.end()[:, :1] / D + 1e-06)
    for i, (at, w) in enumerate(chunks):
        both = scatters[i].end() * scale2
        halls[i][place.kv] = (jax.nn.silu(both[:, :w]) * both[:, w:]).astype(BF16)
        gathers[i].start()
        if i:
            gathers[i - 1].relay()
    loads[3].wait()
    for i, (at, w) in enumerate(chunks):
        if i == n - 1:
            gathers[i].relay()
        gathers[i].end()
        part = jnp.dot(halls[i][...].reshape(wide_n, w), w_down[at:at + w, :], preferred_element_type=F32)
        total[...] = part if i == 0 else total[...] + part
    down = scatter_tp(total[...], d_out, d_in, l_s, l_r)
    out[...] = (mine[...].astype(F32) + down).astype(BF16)
    place.finish()


def column_chunks(width):
    unit = 256 if width % 256 == 0 else 128
    count = width // unit
    parts = min(4, count)
    chunks, at = [], 0
    for i in range(parts):
        w = unit * (count // parts + (1 if i < count % parts else 0))
        chunks.append((at, w))
        at += w
    return chunks


def shards(nkv, ntp, tokens, norm_gain, w_query, w_key, w_value, w_outgate, w_input_gate, w_forget_gate,
           memory, normalizer, stabilizer, w_mix_out, ffn_gain, w_gate, w_up, w_down):
    rows, cw = tokens.shape
    own = rows // nkv
    ny = nkv // 2
    depth = norm_gain.shape[0]
    local_heads = memory.shape[1]
    nh = w_input_gate.shape[1]
    weights = (w_query, w_key, w_value, w_outgate, w_input_gate, w_forget_gate)
    any_spec = pl.BlockSpec(memory_space=pl.ANY)
    vm = pl.BlockSpec(memory_space=pltpu.VMEM)
    dma = pltpu.SemaphoreType.DMA
    widths = [w.shape[1] for w in weights[:4]]
    small = 128
    scratch = [pltpu.VMEM(w.shape, BF16) for w in weights]
    scratch += [pltpu.VMEM((ntp, rows, cw), BF16), pltpu.VMEM((rows, depth), BF16), dma((6,)), dma((ntp,)), dma((ntp,))]
    for n in widths:
        scratch += scatter_scratch(nkv, own, n, BF16)
    scratch += scatter_scratch(nkv, own, small, F32)
    scratch += scatter_sems(5, ny)
    z_query, z_key, z_value, z_outgate, z_small = pl.pallas_call(
        functools.partial(project_kernel, nkv, ntp),
        out_shape=[jax.ShapeDtypeStruct((own, n), F32) for n in widths + [small]],
        in_specs=[vm, vm] + [any_spec] * 6,
        out_specs=[vm] * 5,
        scratch_shapes=scratch,
        compiler_params=pltpu.CompilerParams(collective_id=0, has_side_effects=True, vmem_limit_bytes=VMEM_LIMIT),
        name="project",
    )(tokens, norm_gain.reshape(1, depth), *weights)

    head_start = lax.axis_index("tp") * local_heads
    scale1 = lax.rsqrt(z_small[:, 2 * nh:2 * nh + 1] / D + 1e-06)
    query = (scale1 * z_query).reshape(own, local_heads, DQK) * DQK ** (-0.5)
    key = (scale1 * z_key).reshape(own, local_heads, DQK)
    value = (scale1 * z_value).reshape(own, local_heads, DV)
    outgate = scale1 * z_outgate
    igate = scale1 * lax.dynamic_slice_in_dim(z_small, head_start, local_heads, 1)
    lforget = jax.nn.log_sigmoid(scale1 * lax.dynamic_slice_in_dim(z_small, nh + head_start, local_heads, 1))
    new_stabilizer = jnp.maximum(lforget + stabilizer, igate)
    decay = jnp.exp(lforget + stabilizer - new_stabilizer)
    inflow = jnp.exp(igate - new_stabilizer)
    new_memory = (
        decay[:, :, None, None] * memory
        + inflow[:, :, None, None] * key[:, :, :, None] * value[:, :, None, :]
    )
    new_normalizer = decay[:, :, None] * normalizer + inflow[:, :, None] * key
    numer = jnp.sum(query[:, :, :, None] * new_memory, axis=2)
    denom = jnp.sum(query * new_normalizer, axis=-1)
    readout = numer / jnp.maximum(jnp.abs(denom), jnp.exp(-new_stabilizer))[:, :, None]
    gated = (jax.nn.sigmoid(outgate) * readout.reshape(own, local_heads * DV)).astype(BF16)

    chunks = column_chunks(w_gate.shape[1])
    n = len(chunks)
    mix_rows = gated.shape[1]
    piece = pltpu.VMEM((ntp, rows, cw), BF16)
    scratch = [pltpu.VMEM(w.shape, BF16) for w in (w_mix_out, w_gate, w_up, w_down)]
    scratch += [pltpu.VMEM((nkv, own, mix_rows), BF16), piece, piece, pltpu.VMEM((rows, cw), BF16), piece,
                pltpu.VMEM((rows, depth), BF16), piece, piece, pltpu.VMEM((rows, w_down.shape[1]), F32), dma((4,))]
    scratch += [dma((ntp,))] * 6
    scratch += scatter_scratch(nkv, own, small, F32)
    for _, w in chunks:
        scratch += scatter_scratch(nkv, own, 2 * w, BF16)
    scratch += [pltpu.VMEM((nkv, own, w), BF16) for _, w in chunks]
    scratch += scatter_sems(n + 1, ny) + scatter_sems(n + 1, ny)
    layer_out = pl.pallas_call(
        functools.partial(mixer_kernel, nkv, ntp, chunks),
        out_shape=jax.ShapeDtypeStruct((rows, cw), BF16),
        in_specs=[vm, vm, vm] + [any_spec] * 4,
        out_specs=vm,
        scratch_shapes=scratch,
        compiler_params=pltpu.CompilerParams(collective_id=1, has_side_effects=True, vmem_limit_bytes=VMEM_LIMIT),
        name="mixer",
    )(gated, tokens, ffn_gain.reshape(1, depth), w_mix_out, w_gate, w_up, w_down)
    return (layer_out, new_memory, new_normalizer, new_stabilizer)


def solution(mesh):
    in_specs = (
        P("grp", ("kv", "tp")),
        P("kv"),
        P("kv", "tp"),
        P("kv", "tp"),
        P("kv", "tp"),
        P("kv", "tp"),
        P("kv", None),
        P("kv", None),
        P(("grp", "kv"), "tp", None, None),
        P(("grp", "kv"), "tp", None),
        P(("grp", "kv"), "tp"),
        P("tp", "kv"),
        P("kv"),
        P("kv", "tp"),
        P("kv", "tp"),
        P("tp", "kv"),
    )
    out_specs = (
        P("grp", ("kv", "tp")),
        P(("grp", "kv"), "tp", None, None),
        P(("grp", "kv"), "tp", None),
        P(("grp", "kv"), "tp"),
    )
    body = functools.partial(shards, mesh.shape["kv"], mesh.shape["tp"])
    return jax.shard_map(body, mesh=mesh, in_specs=in_specs, out_specs=out_specs, check_vma=False)
```

time: 283 us -> 77 us (0.27)
  waiting for transfers between devices: 177 us -> 0 us
  Pallas kernels: 0 us -> 54.5 us
  blocking collectives: 45.3 us -> 0 us
  matrix products: 29.1 us -> 0 us
  between operations: 14.6 us -> 0.7 us
  local copies, waits for them, and re-layouts: 3.59 us -> 8.91 us
    reduce_scatter x8 -> x0, waiting for transfers between devices: 143 us -> none  [the longest x6 105 us: shards(): lax.psum_scatter(totals, 'kv', scatter_dimension=0, tiled=True)]
    pallas_call x0 -> x2, Pallas kernels: none -> 54.5 us  [the longest x1 36.6 us: shards(): pl.pallas_call(functools.partial(mixer_kernel, nkv, ntp, chunks), out_sha...]
    all_gather x3 -> x0, blocking collectives: 34.1 us -> none  [the longest x1 15.3 us: shards(): wide = lax.all_gather(tokens, 'tp', axis=1, tiled=True).astype(jnp.float32)]
    psum x1 -> x0, waiting for transfers between devices: 33.5 us -> none  [shards(): lax.psum((gate_part, up_part, square_part), 'kv')]
    dot_general x11 -> x0, matrix products: 29.1 us -> none  [the longest x6 11.6 us: shards(): jnp.dot(normed, weight, preferred_element_type=jnp.float32)]
    reduce_sum x2 -> x1, other arithmetic: 0.25 us -> 6.13 us  [shards(): numer = jnp.sum(query[:, :, :, None] * new_memory, axis=2)]
    psum x1 -> x0, blocking collectives: 5.66 us -> none  [shards(): lax.psum((gate_part, up_part, square_part), 'kv')]
    unnamed x1 -> x0, blocking collectives: 5.63 us -> none
  transfers between devices with their start and end apart: 9 -> 0, of which waited for: 9 -> 0; matrix products, arithmetic and copies ran while one was open for 7% -> 0% of each run, Pallas kernels for 0% -> 0%
where the time goes in v1:
time: 77 us; the launch traced here: 76.1 us
  Pallas kernels  54.5 us (71%)
  other arithmetic  12 us (16%)
  local copies, waits for them, and re-layouts  8.91 us (12%)
    pallas_call x1, Pallas kernels, shards(): pl.pallas_call(functools.partial(mixer_kernel, nkv, ntp, chunks), out_sha...  36.6 us
    pallas_call x1, Pallas kernels, shards(): pl.pallas_call(functools.partial(project_kernel, nkv, ntp), out_shape=[ja...  18 us
    unnamed x10, local copies, waits for them, and re-layouts  6.17 us
    reduce_sum x1, other arithmetic, shards(): numer = jnp.sum(query[:, :, :, None] * new_memory, axis=2)  6.13 us

profile of v1, /device:TPU:0, one launch (start us, length us, event | category | flops | bytes accessed | tf_op | source)
XLA Modules:
  0.0 76.1 jit_solution(13165961787522296800)
XLA Ops:
  0.6 0.0 copy-start.1
  0.6 1.3 %reshape.42.gain = bf16[1,1024]{1,0:T(2,128)(2,1)} reshape(bf16[1024]{0:T(1024)(128)(2,1)} %param.17) | data formatting | bytes 4096 | tf_op jit(solution)/shard_map/reshape | solution.py:317
  2.0 1.3 %reshape.43.gain = bf16[1,1024]{1,0:T(2,128)(2,1)} reshape(bf16[1024]{0:T(1024)(128)(2,1)} %param.28) | data formatting | bytes 4096 | tf_op jit(solution)/shard_map/reshape | solution.py:361
  3.2 0.8 copy.26
  4.0 1.7 %copy.24.refs_4_ = bf16[1024,32]{1,0:T(8,128)(2,1)} copy(bf16[1024,32]{0,1:T(8,128)(2,1)} %param.22) | data formatting | bytes 131072 | tf_op args[6]
  5.7 1.7 %copy.25.refs_5_ = bf16[1024,32]{1,0:T(8,128)(2,1)} copy(bf16[1024,32]{0,1:T(8,128)(2,1)} %param.23) | data formatting | bytes 131072 | tf_op args[7]
  7.3 18.0 %project.1 = (f32[16,512]{1,0:T(8,128)}, f32[16,512]{1,0:T(8,128)}, f32[16,1024]{1,0:T(8,128)}, f32[16,1024]{1,0:T(8,128)}, f32[16,128]{1,0:T(8,128)}) custom-call(bf16[64,256]{1,0:T(8,128)(2,1)} %tokens.3, bf16[1,1024]{1,0:T(2,128)(2,1)} %reshape.42.gain, bf16[1024,512]{1,0:T(8,128)(2,1)} %refs_0_.2, bf16[1024,512]{1,0:T(8,128)(2,1)} %refs_1_.2, ...), custom_call_target="tpu_custom_call" | custom-call | tf_op jit(solution)/shard_map/project/pallas_call | solution.py:309
  25.3 0.9 %rsqrt_reduce_fusion = f32[16]{0:T(128)S(1)} fusion(f32[16,128]{1,0:T(8,128)} %get-tuple-element.9), kind=kLoop, calls=%fused_computation.18 | loop fusion | flops 32 | bytes 128 | tf_op jit(solution)/shard_map/rsqrt | solution.py:320
  26.2 0.9 %multiply_bitcast_fusion = f32[2,8,8,128]{3,1,2,0:T(8,128)S(1)} fusion(f32[16,1024]{1,0:T(8,128)} %get-tuple-element.13, f32[16]{0:T(128)S(1)} %rsqrt_reduce_fusion), kind=kLoop, calls=%fused_computation.6 | loop fusion | flops 16384 | bytes 131136
  27.1 0.9 %broadcast_multiply_fusion.1 = (f32[16,512]{1,0:T(8,128)S(1)}, f32[16,512]{1,0:T(8,128)S(1)}) fusion(f32[16,512]{1,0:T(8,128)} %get-tuple-element.12, f32[16]{0:T(128)S(1)} %rsqrt_reduce_fusion, f32[16,512]{1,0:T(8,128)} %get-tuple-element.11), kind=kLoop, calls=%fused_computation.11 | loop fusion | flops 24576 | bytes 131136 | tf_op jit(solution)/shard_map/mul | solution.py:322
  28.0 0.9 %subtract_exponential_fusion.1 = (f32[16,8]{1,0:T(8,128)S(1)}, f32[16,8]{1,0:T(8,128)S(1)}) fusion(f32[16,8]{1,0:T(8,128)S(1)} %copy.26, f32[16,128]{1,0:T(8,128)} %get-tuple-element.9, s32[]{:T(128)S(6)} %select_n.11, f32[16]{0:T(128)S(1)} %rsqrt_reduce_fusion, s32[]{:T(128)S(6)} %select_n.13), kind=kLoop, calls=%fused_computation.16 | loop fusion | flops 1664 | bytes 2632 | tf_op jit(solution)/shard_map/exp | solution.py:328
  28.9 0.8 %subtract_exponential_fusion = f32[16,8]{1,0:T(8,128)S(1)} fusion(f32[16,8]{1,0:T(8,128)S(1)} %get-tuple-element.28, f32[16,128]{1,0:T(8,128)} %get-tuple-element.9, s32[]{:T(128)S(6)} %select_n.13, f32[16]{0:T(128)S(1)} %rsqrt_reduce_fusion), kind=kLoop, calls=%fused_computation.15 | loop fusion | flops 256 | bytes 1604 | tf_op jit(solution)/shard_map/exp | solution.py:329
  29.7 0.7 copy.27
  30.3 0.1 broadcast_in_dim_reshape.4
  30.4 0.1 mul.129
  30.5 0.0 copy-done.1
  30.5 0.7 multiply_reduce_fusion.1
  31.2 0.0 copy-start
  31.2 6.1 %multiply_reduce_fusion = (f32[16,8,128]{2,1,0:T(8,128)S(1)}, f32[16,8,64,128]{3,2,1,0:T(8,128)}) fusion(f32[16,8,64]{2,1,0:T(8,128)S(1)} %mul.129, f32[16,8,128]{2,1,0:T(8,128)S(1)} %bitcast.8, f32[16,8,64]{2,1,0:T(8,128)S(1)} %get-tuple-element.24, f32[16,8,64,128]{3,2,1,0:T(8,128)} %param.24, f32[16,8]{1,0:T(8,128)S(1)} %get-tuple-element.27), kind=kLoop, calls=%fused_computation | loop fusion | flops 5226496 | bytes 8585728 | tf_op jit(solution)/shard_map/reduce_sum | solution.py:335
  37.4 0.1 broadcast_divide_fusion
  37.5 0.0 copy-done
  37.5 0.7 fusion.gated
  38.2 36.6 %mixer.1 = bf16[64,256]{1,0:T(8,128)(2,1)} custom-call(bf16[16,1024]{1,0:T(8,128)(2,1)} %fusion.gated, bf16[64,256]{1,0:T(8,128)(2,1)} %tokens.3, bf16[1,1024]{1,0:T(2,128)(2,1)} %reshape.43.gain, bf16[1024,1024]{1,0:T(8,128)(2,1)} %refs_0_.3, bf16[1024,2816]{1,0:T(8,128)(2,1)} %refs_1_.3, bf16[1024,2816]{1,0:T(8,128)(2,1)} %refs_2_.3, ...), custom_call_target="tpu_custom_call" | custom-call | tf_op jit(solution)/shard_map/mixer/pallas_call | solution.py:353
  74.7 1.4 %copy.32 = bf16[64,256]{1,0:T(8,128)(2,1)} copy(bf16[64,256]{1,0:T(8,128)(2,1)} %mixer.1) | data formatting | bytes 65536
  (2 shorter events, 0.0 us)
Async XLA Ops:
  0.6 29.8 %copy-start.1 = (f32[16,8,64]{2,1,0:T(8,128)S(1)}, f32[16,8,64]{2,1,0:T(8,128)}, u32[]{:S(2)}) copy-start(f32[16,8,64]{2,1,0:T(8,128)} %param.25) | copy-start | bytes 98308
  31.2 6.2 %copy-start = (f32[16,1024]{1,0:T(8,128)S(1)}, f32[16,1024]{1,0:T(8,128)}, u32[]{:S(2)}) copy-start(f32[16,1024]{1,0:T(8,128)} %get-tuple-element.10) | copy-start | bytes 196612

commit v2 on v1

--- a/solution.py
+++ b/solution.py
@@ -145,10 +145,11 @@
 
 def normalize(place, pieces, gain, normed):
     cw = pieces.shape[2]
+    gain = gain[...].astype(F32).reshape(1, gain.shape[0])
     squares = None
     for t in range(place.ntp):
         wide = pieces[t].astype(F32)
-        normed[:, t * cw:(t + 1) * cw] = (wide * gain[:, t * cw:(t + 1) * cw].astype(F32)).astype(BF16)
+        normed[:, t * cw:(t + 1) * cw] = (wide * gain[:, t * cw:(t + 1) * cw]).astype(BF16)
         part = jnp.sum(wide * wide, axis=1, keepdims=True)
         squares = part if squares is None else squares + part
     return squares
@@ -179,11 +180,12 @@
         return value.reshape(nkv, own, value.shape[1])
 
     small = groups[16]
-    nh = vmem[4].shape[1]
+    nh = vmem[4].shape[0]
     small[:, :, 2 * nh:] = split(jnp.broadcast_to(squares, (nkv * own, small.shape[2] - 2 * nh)))
     for g, at in ((4, 0), (5, nh)):
         loads[g].wait()
-        small[:, :, at:at + nh] = split(jnp.dot(normed[...], vmem[g][...], preferred_element_type=F32))
+        small[:, :, at:at + nh] = split(lax.dot_general(
+            normed[...], vmem[g][...], (((1,), (1,)), ((), ())), preferred_element_type=F32))
     scatters[4].start()
     for g in range(4):
         loads[g].wait()
@@ -194,6 +196,48 @@
     for g in (4, 0, 1, 2, 3):
         outs[g][...] = scatters[g].end()
     place.finish()
+
+
+def state_kernel(nh, ntp, zq, zk, zv, zo, zs, normalizer, stabilizer, memory,
+                 new_memory, new_normalizer, new_stabilizer, gated, old, new, in_sem, out_sem):
+    heads, own = stabilizer.shape
+    loads = [pltpu.make_async_copy(memory.at[:, h], old.at[h], in_sem.at[h]) for h in range(heads)]
+    for copy in loads:
+        copy.start()
+    tp = lax.axis_index("tp")
+    scale1 = lax.rsqrt(zs[:, 2 * nh:2 * nh + 1] / D + 1e-06)
+
+    def own_heads(at):
+        value = zs[:, at:at + heads]
+        for t in range(1, ntp):
+            value = jnp.where(tp == t, zs[:, at + t * heads:at + (t + 1) * heads], value)
+        return scale1 * value
+
+    igate, forget = own_heads(0), own_heads(nh)
+    lforget = jnp.minimum(forget, 0.0) - jnp.log1p(jnp.exp(-jnp.abs(forget)))
+    kept = lforget + stabilizer[...].T
+    stab = jnp.maximum(kept, igate)
+    new_stabilizer[...] = stab.T
+    decay, inflow, floor = jnp.exp(kept - stab), jnp.exp(igate - stab), jnp.exp(-stab)
+    stores = []
+    for h in range(heads):
+        query = scale1 * zq[:, h * DQK:(h + 1) * DQK] * DQK ** (-0.5)
+        key = inflow[:, h:h + 1] * (scale1 * zk[:, h * DQK:(h + 1) * DQK])
+        value = scale1 * zv[:, h * DV:(h + 1) * DV]
+        norm = decay[:, h:h + 1] * normalizer[:, h, :] + key
+        new_normalizer[:, h, :] = norm
+        denom = jnp.maximum(jnp.abs(jnp.sum(query * norm, axis=1, keepdims=True)), floor[:, h:h + 1])
+        loads[h].wait()
+        wide = jnp.broadcast_to(decay[:, h:h + 1], (own, DV))
+        state = wide[:, None, :] * old[h] + key[:, :, None] * value[:, None, :]
+        new[h] = state
+        stores.append(pltpu.make_async_copy(new.at[h], new_memory.at[:, h], out_sem.at[h]))
+        stores[h].start()
+        numer = jnp.sum(query[:, :, None] * state, axis=1)
+        out = jax.nn.sigmoid(scale1 * zo[:, h * DV:(h + 1) * DV]) * (numer / denom)
+        gated[:, h * DV:(h + 1) * DV] = out.astype(BF16)
+    for copy in stores:
+        copy.wait()
 
 
 def mixer_kernel(nkv, ntp, chunks, gated, tokens, gain, *refs):
@@ -294,7 +338,7 @@
     depth = norm_gain.shape[0]
     local_heads = memory.shape[1]
     nh = w_input_gate.shape[1]
-    weights = (w_query, w_key, w_value, w_outgate, w_input_gate, w_forget_gate)
+    weights = (w_query, w_key, w_value, w_outgate, w_input_gate.T, w_forget_gate.T)
     any_spec = pl.BlockSpec(memory_space=pl.ANY)
     vm = pl.BlockSpec(memory_space=pltpu.VMEM)
     dma = pltpu.SemaphoreType.DMA
@@ -314,28 +358,29 @@
         scratch_shapes=scratch,
         compiler_params=pltpu.CompilerParams(collective_id=0, has_side_effects=True, vmem_limit_bytes=VMEM_LIMIT),
         name="project",
-    )(tokens, norm_gain.reshape(1, depth), *weights)
-
-    head_start = lax.axis_index("tp") * local_heads
-    scale1 = lax.rsqrt(z_small[:, 2 * nh:2 * nh + 1] / D + 1e-06)
-    query = (scale1 * z_query).reshape(own, local_heads, DQK) * DQK ** (-0.5)
-    key = (scale1 * z_key).reshape(own, local_heads, DQK)
-    value = (scale1 * z_value).reshape(own, local_heads, DV)
-    outgate = scale1 * z_outgate
-    igate = scale1 * lax.dynamic_slice_in_dim(z_small, head_start, local_heads, 1)
-    lforget = jax.nn.log_sigmoid(scale1 * lax.dynamic_slice_in_dim(z_small, nh + head_start, local_heads, 1))
-    new_stabilizer = jnp.maximum(lforget + stabilizer, igate)
-    decay = jnp.exp(lforget + stabilizer - new_stabilizer)
-    inflow = jnp.exp(igate - new_stabilizer)
-    new_memory = (
-        decay[:, :, None, None] * memory
-        + inflow[:, :, None, None] * key[:, :, :, None] * value[:, :, None, :]
-    )
-    new_normalizer = decay[:, :, None] * normalizer + inflow[:, :, None] * key
-    numer = jnp.sum(query[:, :, :, None] * new_memory, axis=2)
-    denom = jnp.sum(query * new_normalizer, axis=-1)
-    readout = numer / jnp.maximum(jnp.abs(denom), jnp.exp(-new_stabilizer))[:, :, None]
-    gated = (jax.nn.sigmoid(outgate) * readout.reshape(own, local_heads * DV)).astype(BF16)
+    )(tokens, norm_gain, *weights)
+
+    hbm = pl.BlockSpec(memory_space=pltpu.HBM)
+    new_memory, new_normalizer, new_stabilizer, gated = pl.pallas_call(
+        functools.partial(state_kernel, nh, ntp),
+        out_shape=[
+            jax.ShapeDtypeStruct(memory.shape, F32),
+            jax.ShapeDtypeStruct(normalizer.shape, F32),
+            jax.ShapeDtypeStruct((local_heads, own), F32),
+            jax.ShapeDtypeStruct((own, local_heads * DV), BF16),
+        ],
+        in_specs=[vm] * 7 + [hbm],
+        out_specs=[hbm, vm, vm, vm],
+        scratch_shapes=[
+            pltpu.VMEM((local_heads, own, DQK, DV), F32),
+            pltpu.VMEM((local_heads, own, DQK, DV), F32),
+            dma((local_heads,)),
+            dma((local_heads,)),
+        ],
+        compiler_params=pltpu.CompilerParams(vmem_limit_bytes=VMEM_LIMIT),
+        name="state",
+    )(z_query, z_key, z_value, z_outgate, z_small, normalizer, stabilizer.T, memory)
+    new_stabilizer = new_stabilizer.T
 
     chunks = column_chunks(w_gate.shape[1])
     n = len(chunks)
@@ -358,7 +403,7 @@
         scratch_shapes=scratch,
         compiler_params=pltpu.CompilerParams(collective_id=1, has_side_effects=True, vmem_limit_bytes=VMEM_LIMIT),
         name="mixer",
-    )(gated, tokens, ffn_gain.reshape(1, depth), w_mix_out, w_gate, w_up, w_down)
+    )(gated, tokens, ffn_gain, w_mix_out, w_gate, w_up, w_down)
     return (layer_out, new_memory, new_normalizer, new_stabilizer)
 
 

time: 77 us -> 63.9 us (0.83)
  other arithmetic: 12 us -> 0 us
  local copies, waits for them, and re-layouts: 8.91 us -> 1.38 us
  Pallas kernels: 54.5 us -> 61.5 us
    reduce_sum x2 -> x0, other arithmetic: 6.87 us -> none  [the longest x1 6.13 us: shards(): numer = jnp.sum(query[:, :, :, None] * new_memory, axis=2)]
    pallas_call x0 -> x1, Pallas kernels: none -> 6.84 us  [shards(): pl.pallas_call(functools.partial(state_kernel, nh, ntp), out_shape=[jax.S...]
    unnamed x10 -> x1, local copies, waits for them, and re-layouts: 6.17 us -> 1.38 us
    reshape x2 -> x0, local copies, waits for them, and re-layouts: 2.58 us -> none  [the longest x1 1.31 us: shards(): norm_gain.reshape(1, depth)]
    exp x2 -> x0, other arithmetic: 1.64 us -> none  [the longest x1 0.87 us: shards(): decay = jnp.exp(lforget + stabilizer - new_stabilizer)]
    unnamed x1 -> x0, other arithmetic: 0.92 us -> none
    rsqrt x1 -> x0, other arithmetic: 0.88 us -> none  [shards(): scale1 = lax.rsqrt(z_small[:, 2 * nh:2 * nh + 1] / D + 1e-06)]
    mul x1 -> x0, other arithmetic: 0.85 us -> none  [shards(): key = (scale1 * z_key).reshape(own, local_heads, DQK)]
where the time goes in v2:
time: 63.9 us; the launch traced here: 63.5 us
  Pallas kernels  61.5 us (96%)
  local copies, waits for them, and re-layouts  1.38 us (2%)
  between operations  0.66 us (1%)
    pallas_call x1, Pallas kernels, shards(): pl.pallas_call(functools.partial(mixer_kernel, nkv, ntp, chunks), out_sha...  36.6 us
    pallas_call x1, Pallas kernels, shards(): pl.pallas_call(functools.partial(project_kernel, nkv, ntp), out_shape=[ja...  18 us
    pallas_call x1, Pallas kernels, shards(): pl.pallas_call(functools.partial(state_kernel, nh, ntp), out_shape=[jax.S...  6.84 us
    unnamed x1, local copies, waits for them, and re-layouts  1.38 us

profile of v2, /device:TPU:0, one launch (start us, length us, event | category | flops | bytes accessed | tf_op | source)
XLA Modules:
  0.0 63.5 jit_solution(1330181196680363687)
XLA Ops:
  0.6 18.0 %project.1 = (f32[16,512]{1,0:T(8,128)}, f32[16,512]{1,0:T(8,128)}, f32[16,1024]{1,0:T(8,128)}, f32[16,1024]{1,0:T(8,128)}, f32[16,128]{1,0:T(8,128)}) custom-call(bf16[64,256]{1,0:T(8,128)(2,1)} %tokens.3, bf16[1024]{0:T(1024)(128)(2,1)} %gain.2, bf16[1024,512]{1,0:T(8,128)(2,1)} %refs_0_.2, bf16[1024,512]{1,0:T(8,128)(2,1)} %refs_1_.2, ...), custom_call_target="tpu_custom_call" | custom-call | tf_op jit(solution)/shard_map/project/pallas_call | solution.py:353
  18.7 6.8 %state.1 = (f32[16,8,64,128]{3,2,1,0:T(8,128)}, f32[16,8,64]{2,1,0:T(8,128)}, f32[8,16]{1,0:T(8,128)}, bf16[16,1024]{1,0:T(8,128)(2,1)}) custom-call(f32[16,512]{1,0:T(8,128)} %get-tuple-element.13.zq, f32[16,512]{1,0:T(8,128)} %get-tuple-element.14.zk, f32[16,1024]{1,0:T(8,128)} %get-tuple-element.15.zv, f32[16,1024]{1,0:T(8,128)} %get-tuple-element.16.zo, ...), custom_call_target="tpu_custom_call" | custom-call | tf_op jit(solution)/shard_map/state/pallas_call | solution.py:364
  25.5 36.6 %mixer.1 = bf16[64,256]{1,0:T(8,128)(2,1)} custom-call(bf16[16,1024]{1,0:T(8,128)(2,1)} %get-tuple-element.18.gated, bf16[64,256]{1,0:T(8,128)(2,1)} %tokens.3, bf16[1024]{0:T(1024)(128)(2,1)} %gain.3, bf16[1024,1024]{1,0:T(8,128)(2,1)} %refs_0_.3, bf16[1024,2816]{1,0:T(8,128)(2,1)} %refs_1_.3, bf16[1024,2816]{1,0:T(8,128)(2,1)} %refs_2_.3, ...), custom_call_target="tpu_custom_call" | custom-call | tf_op jit(solution)/shard_map/mixer/pallas_call | solution.py:398
  62.1 1.4 %copy.21 = bf16[64,256]{1,0:T(8,128)(2,1)} copy(bf16[64,256]{1,0:T(8,128)(2,1)} %mixer.1) | data formatting | bytes 65536

commit v3 on v2

--- a/solution.py
+++ b/solution.py
@@ -191,8 +191,8 @@
         loads[g].wait()
         groups[4 * g][...] = split(jnp.dot(normed[...], vmem[g][...], preferred_element_type=F32))
         scatters[g].start()
-        scatters[g - 1 if g else 4].middle()
-    scatters[3].middle()
+    for g in (4, 0, 1, 2, 3):
+        scatters[g].middle()
     for g in (4, 0, 1, 2, 3):
         outs[g][...] = scatters[g].end()
     place.finish()
@@ -304,12 +304,10 @@
         both = scatters[i].end() * scale2
         halls[i][place.kv] = (jax.nn.silu(both[:, :w]) * both[:, w:]).astype(BF16)
         gathers[i].start()
-        if i:
-            gathers[i - 1].relay()
     loads[3].wait()
+    for gather in gathers:
+        gather.relay()
     for i, (at, w) in enumerate(chunks):
-        if i == n - 1:
-            gathers[i].relay()
         gathers[i].end()
         part = jnp.dot(halls[i][...].reshape(wide_n, w), w_down[at:at + w, :], preferred_element_type=F32)
         total[...] = part if i == 0 else total[...] + part

time: 63.9 us -> 61.7 us (0.966)
  Pallas kernels: 61.5 us -> 59.3 us
    pallas_call x1, Pallas kernels: 36.6 us -> 35 us  [shards(): pl.pallas_call(functools.partial(mixer_kernel, nkv, ntp, chunks), out_sha...]
where the time goes in v3:
time: 61.7 us; the launch traced here: 61.3 us
  Pallas kernels  59.3 us (96%)
  local copies, waits for them, and re-layouts  1.38 us (2%)
  between operations  0.66 us (1%)
    pallas_call x1, Pallas kernels, shards(): pl.pallas_call(functools.partial(mixer_kernel, nkv, ntp, chunks), out_sha...  35 us
    pallas_call x1, Pallas kernels, shards(): pl.pallas_call(functools.partial(project_kernel, nkv, ntp), out_shape=[ja...  17.5 us
    pallas_call x1, Pallas kernels, shards(): pl.pallas_call(functools.partial(state_kernel, nh, ntp), out_shape=[jax.S...  6.84 us
    unnamed x1, local copies, waits for them, and re-layouts  1.38 us

profile of v3, /device:TPU:0, one launch (start us, length us, event | category | flops | bytes accessed | tf_op | source)
XLA Modules:
  0.0 61.3 jit_solution(7126147539970196536)
XLA Ops:
  0.6 17.5 %project.1 = (f32[16,512]{1,0:T(8,128)}, f32[16,512]{1,0:T(8,128)}, f32[16,1024]{1,0:T(8,128)}, f32[16,1024]{1,0:T(8,128)}, f32[16,128]{1,0:T(8,128)}) custom-call(bf16[64,256]{1,0:T(8,128)(2,1)} %tokens.3, bf16[1024]{0:T(1024)(128)(2,1)} %gain.2, bf16[1024,512]{1,0:T(8,128)(2,1)} %refs_0_.2, bf16[1024,512]{1,0:T(8,128)(2,1)} %refs_1_.2, ...), custom_call_target="tpu_custom_call" | custom-call | tf_op jit(solution)/shard_map/project/pallas_call | solution.py:351
  18.2 6.8 %state.1 = (f32[16,8,64,128]{3,2,1,0:T(8,128)}, f32[16,8,64]{2,1,0:T(8,128)}, f32[8,16]{1,0:T(8,128)}, bf16[16,1024]{1,0:T(8,128)(2,1)}) custom-call(f32[16,512]{1,0:T(8,128)} %get-tuple-element.13.zq, f32[16,512]{1,0:T(8,128)} %get-tuple-element.14.zk, f32[16,1024]{1,0:T(8,128)} %get-tuple-element.15.zv, f32[16,1024]{1,0:T(8,128)} %get-tuple-element.16.zo, ...), custom_call_target="tpu_custom_call" | custom-call | tf_op jit(solution)/shard_map/state/pallas_call | solution.py:362
  25.0 35.0 %mixer.1 = bf16[64,256]{1,0:T(8,128)(2,1)} custom-call(bf16[16,1024]{1,0:T(8,128)(2,1)} %get-tuple-element.18.gated, bf16[64,256]{1,0:T(8,128)(2,1)} %tokens.3, bf16[1024]{0:T(1024)(128)(2,1)} %gain.3, bf16[1024,1024]{1,0:T(8,128)(2,1)} %refs_0_.3, bf16[1024,2816]{1,0:T(8,128)(2,1)} %refs_1_.3, bf16[1024,2816]{1,0:T(8,128)(2,1)} %refs_2_.3, ...), custom_call_target="tpu_custom_call" | custom-call | tf_op jit(solution)/shard_map/mixer/pallas_call | solution.py:396
  60.0 1.4 %copy.21 = bf16[64,256]{1,0:T(8,128)(2,1)} copy(bf16[64,256]{1,0:T(8,128)(2,1)} %mixer.1) | data formatting | bytes 65536
